TPU v7x, 32 devices: a whole 2x2x4 slice. The times are simulated.
32 devices in a mesh: sp: 8 (over z, y), tp: 4 (over x, core).
Axes of the slice: x: 2, y: 2, z: 4, core: 2. Of those that a mesh axis runs over, the one named last changes fastest.
Arguments:
- tokens: bfloat16 [6144, 2048], P('sp', 'tp'), may hold values from -18 to 18
- proj_weight: bfloat16 [2048, 1024], P(None, 'tp'), may hold values from -0.125 to 0.125
- gate_weight: bfloat16 [2048, 1024], P(None, 'tp'), may hold values from -0.125 to 0.125
- conv_weight: float32 [4, 1024], replicated, may hold values from -3 to 3
- recur_weight: bfloat16 [16, 64, 64], replicated, may hold values from -0.75 to 0.75
- input_weight: bfloat16 [16, 64, 64], replicated, may hold values from -0.75 to 0.75
- decay_param: float32 [1024], replicated, as said below
- out_grad: bfloat16 [6144, 1024], P('sp', 'tp'), may hold values from -6 to 6
Outputs:
- d_proj: bfloat16 [6144, 1024], P('sp', 'tp')
- d_gate: bfloat16 [6144, 1024], P('sp', 'tp')
- d_weight: float32 [2048, 1024], P('sp', 'tp')
Inputs may be any that keep to these rules, and one draw needn't show every extreme that they name: `decay_param`: every channel's decay parameter is at least 4; there is no fixed upper bound.
All inputs are finite; a program needn't handle non-finite values.
Results may differ from a plain program's by a relative error of at most 0.01.
Values may be sent and summed in bfloat16 or wider, within the bound.
A program may use at most 64 MiB of HBM per device.

v0:
```python
import jax
import jax.numpy as jnp
from jax import lax
from jax.sharding import PartitionSpec as P

BLOCK = 64
rate_scale = 8.0
scale_floor = 0.0001


def from_behind(value, axis, steps):
    count = lax.axis_size(axis)
    first, last = (max(0, -steps), min(count, count - steps))
    return lax.ppermute(value, axis, [(source, source + steps) for source in range(first, last)])


def combine(earlier, later):
    return (earlier[0] * later[0], later[0] * earlier[1] + later[1])


def block_map(values, weights, block_count):
    row_count = values.shape[0]
    shaped = values.reshape(row_count, block_count, BLOCK)
    result = jnp.einsum("tgi,gij->tgj", shaped, weights, preferred_element_type=jnp.float32)
    return result.reshape(row_count, block_count * BLOCK)


def block_back(values, weights, block_count):
    row_count = values.shape[0]
    shaped = values.reshape(row_count, block_count, BLOCK)
    result = jnp.einsum("tgj,gij->tgi", shaped, weights, preferred_element_type=jnp.float32)
    return result.reshape(row_count, block_count * BLOCK)


def per_device(
    tokens, proj_weight, gate_weight, conv_weight, recur_weight, input_weight, decay_param, out_grad
):
    tp_index = lax.axis_index("tp")
    row_count = tokens.shape[0]
    chan_width = proj_weight.shape[1]
    block_count = chan_width // BLOCK
    gathered = lax.all_gather(tokens, "tp", axis=1, tiled=True)
    projected = jnp.dot(gathered, proj_weight, preferred_element_type=jnp.float32).astype(
        jnp.bfloat16
    )
    gate_in = jnp.dot(gathered, gate_weight, preferred_element_type=jnp.float32).astype(
        jnp.bfloat16
    )
    conv_taps = lax.dynamic_slice_in_dim(conv_weight, tp_index * chan_width, chan_width, 1)
    decay_slice = lax.dynamic_slice_in_dim(decay_param, tp_index * chan_width, chan_width, 0)
    w_recur = lax.dynamic_slice_in_dim(recur_weight, tp_index * block_count, block_count, 0)
    w_input = lax.dynamic_slice_in_dim(input_weight, tp_index * block_count, block_count, 0)
    prior_rows = from_behind(projected[row_count - 3 :], "sp", 1)
    padded = jnp.concatenate([prior_rows, projected], axis=0).astype(jnp.float32)
    total = conv_taps[0] * padded[3 : 3 + row_count]
    for offset in range(1, 4):
        total = total + conv_taps[offset] * padded[3 - offset : 3 - offset + row_count]
    conv_out = total.astype(jnp.bfloat16)
    conv_float = conv_out.astype(jnp.float32)
    recur_open = jax.nn.sigmoid(block_map(conv_out, w_recur, block_count))
    input_open = jax.nn.sigmoid(block_map(conv_out, w_input, block_count))
    log_slope = rate_scale * jax.nn.log_sigmoid(decay_slice)
    log_decay = log_slope * recur_open
    decay_rate = jnp.exp(log_decay)
    input_scale = jnp.sqrt(scale_floor - jnp.expm1(2.0 * log_decay))
    gated_input = input_open * conv_float
    drive = input_scale * gated_input
    cum_decay, local_states = lax.associative_scan(combine, (decay_rate, drive), axis=0)
    gelu_gate, gelu_back = jax.vjp(jax.nn.gelu, gate_in.astype(jnp.float32))
    cotangent = out_grad.astype(jnp.float32)
    drive_grad = cotangent * gelu_gate
    shifted = jnp.concatenate([decay_rate[1:], jnp.ones((1, chan_width), jnp.float32)], axis=0)
    cum_after, local_grad = lax.associative_scan(
        combine, (shifted, drive_grad), reverse=True, axis=0
    )
    span_decay = cum_decay[-1]
    span_state = local_states[-1]
    span_grad = decay_rate[0] * local_grad[0]
    all_decay, all_state, all_grad = (
        lax.all_gather(span_decay[None], "sp", axis=0, tiled=True),
        lax.all_gather(span_state[None], "sp", axis=0, tiled=True),
        lax.all_gather(span_grad[None], "sp", axis=0, tiled=True),
    )
    sp_index = lax.axis_index("sp")
    sp_count = lax.axis_size("sp")
    _, fwd_state = lax.associative_scan(combine, (all_decay, all_state), axis=0)
    _, rev_grad = lax.associative_scan(combine, (all_decay, all_grad), reverse=True, axis=0)
    before = lax.dynamic_index_in_dim(fwd_state, jnp.maximum(sp_index - 1, 0), 0, False)
    after = lax.dynamic_index_in_dim(rev_grad, jnp.minimum(sp_index + 1, sp_count - 1), 0, False)
    carry_state = jnp.where(sp_index > 0, before, 0.0)
    carry_grad = jnp.where(sp_index < sp_count - 1, after, 0.0)
    states = local_states + cum_decay * carry_state
    previous = jnp.concatenate([carry_state[None], states[:-1]], axis=0)
    d_gate = gelu_back(cotangent * states)[0].astype(jnp.bfloat16)
    state_grad = local_grad + cum_after * carry_grad
    d_log_decay = state_grad * (
        decay_rate * previous - gated_input * decay_rate * decay_rate / input_scale
    )
    d_recur_pre = (d_log_decay * log_slope * recur_open * (1.0 - recur_open)).astype(jnp.bfloat16)
    d_input_pre = (state_grad * input_scale * conv_float * input_open * (1.0 - input_open)).astype(
        jnp.bfloat16
    )
    d_conv = state_grad * input_scale * input_open
    d_conv = d_conv + block_back(d_recur_pre, w_recur, block_count)
    d_conv = d_conv + block_back(d_input_pre, w_input, block_count)
    next_rows = from_behind(d_conv[:3], "sp", -1)
    extended = jnp.concatenate([d_conv, next_rows], axis=0)
    grad_sum = conv_taps[0] * extended[0:row_count]
    for offset in range(1, 4):
        grad_sum = grad_sum + conv_taps[offset] * extended[offset : offset + row_count]
    d_proj = grad_sum.astype(jnp.bfloat16)
    d_weight = lax.psum_scatter(
        lax.dot_general(
            gathered, d_proj, (((0,), (0,)), ((), ())), preferred_element_type=jnp.float32
        ),
        "sp",
        scatter_dimension=0,
        tiled=True,
    )
    return (d_proj, d_gate, d_weight)


def solution(mesh):
    in_specs = (P("sp", "tp"), P(None, "tp"), P(None, "tp"), P(), P(), P(), P(), P("sp", "tp"))
    out_specs = (P("sp", "tp"), P("sp", "tp"), P("sp", "tp"))
    return jax.shard_map(
        per_device, mesh=mesh, in_specs=in_specs, out_specs=out_specs, check_vma=False
    )
```

profile of v0, /device:TPU:0, one launch (start us, length us, event | category | flops | bytes accessed | tf_op | source)
XLA Modules:
  0.0 441.6 jit_solution(7558327511127030171)
XLA Ops:
  8.9 31.9 %all-gather.5.cloned.1.call-done = bf16[768,2048]{1,0:T(8,128)(2,1)} async-done(((bf16[768,512]{1,0:T(8,128)(2,1)}), bf16[768,2048]{1,0:T(8,128)(2,1)}) %all-gather.5.cloned.1.call-update) | async-done | bytes 3145744 | tf_op jit(solution)/shard_map/all_gather | solution.py:42
  40.8 3.1 convolution_convert_fusion
  44.0 3.4 collective-permute-start
  57.1 3.2 slice.964
  60.3 3.2 slice.924
  63.5 3.2 slice.923
  168.3 2.5 pad.335
  177.2 2.5 fusion.40
  180.5 2.9 pad.336
  183.4 3.0 pad.337
  187.1 21.3 %all-gather.2 = f32[8,1,256]{2,1,0:T(1,128)S(1)} all-gather(f32[1,1,256]{2,1,0:T(1,128)S(1)} %add_bitcast_fusion), channel_id=1, replica_groups=mesh['sp'=8,'tp'=4] {'sp'}, dimensions={0}, use_global_device_ids=true | all-gather | bytes 9216 | tf_op jit(solution)/shard_map/all_gather | solution.py:81
  210.2 2.9 pad.312
  213.2 2.9 pad.313
  216.7 16.5 %all-gather.1 = f32[8,1,256]{2,1,0:T(1,128)S(1)} all-gather(f32[1,1,256]{2,1,0:T(1,128)S(1)} %add_bitcast_fusion.1), channel_id=1, replica_groups=mesh['sp'=8,'tp'=4] {'sp'}, dimensions={0}, use_global_device_ids=true | all-gather | bytes 9216 | tf_op jit(solution)/shard_map/all_gather | solution.py:80
  233.7 5.5 %fusion.12 = (bf16[768,256]{1,0:T(8,128)(2,1)}, f32[768,256]{1,0:T(8,128)}, f32[768,256]{1,0:T(8,128)S(1)}) fusion(bf16[768,256]{1,0:T(8,128)(2,1)} %param.15, f32[256]{0:T(256)S(1)} %bitcast.89, f32[768,256]{1,0:T(8,128)} %pad.312, f32[768,256]{1,0:T(8,128)} %pad.313, f32[768,256]{1,0:T(8,128)} %pad.336, f32[768,256]{1,0:T(8,128)} %pad.337, ...), kind=kOutput, calls=%fused_computation.29 | convolution fusion | flops 811204608 | bytes 9700352 | tf_op jit(solution)/shard_map/dot_general | solution.py:46
  240.1 3.2 slice.834
  243.3 3.1 slice.768
  246.4 3.1 slice.766
  254.1 3.9 slice.767
  258.0 3.8 slice.769
  261.8 3.8 slice.772
  265.6 3.8 slice.765
  280.8 4.0 slice.763
  294.9 2.5 pad.275
  305.2 3.0 pad.277
  310.1 18.3 %all-gather = f32[8,1,256]{2,1,0:T(1,128)S(1)} all-gather(f32[1,1,256]{2,1,0:T(1,128)S(1)} %fusion.85), channel_id=1, replica_groups=mesh['sp'=8,'tp'=4] {'sp'}, dimensions={0}, use_global_device_ids=true | all-gather | bytes 9216 | tf_op jit(solution)/shard_map/all_gather | solution.py:82
  331.4 2.9 pad.294
  334.3 3.0 pad.295
  339.6 6.8 %rev.14 = f32[768,256]{1,0:T(8,128)} reverse(f32[768,256]{1,0:T(8,128)} %add.556), dimensions={0} | reverse | bytes 1572864 | tf_op jit(solution)/shard_map/rev | solution.py:73
  346.5 3.7 fusion.9
  360.0 4.2 collective-permute-done.1
  366.9 66.0 %reduce-scatter.2.cloned.1.call-done = f32[256,256]{0,1:T(8,128)} async-done(((f32[2048,256]{0,1:T(8,128)}), f32[256,256]{0,1:T(8,128)}) %reduce-scatter.2.cloned.1.call-update) | async-done | bytes 262160 | tf_op jit(solution)/shard_map/reduce_scatter | solution.py:112
  (439 shorter events, 179.1 us)
Async XLA Ops:
  7.2 226.6 %copy-start = (bf16[2048,256]{1,0:T(8,128)(2,1)S(1)}, bf16[2048,256]{1,0:T(8,128)(2,1)}, u32[]{:S(2)}) copy-start(bf16[2048,256]{1,0:T(8,128)(2,1)} %param.10) | copy-start | bytes 3145732
  7.2 33.6 %all-gather.5.cloned.1.call-start = ((), (), s32[]{:S(2)}) async-start(), calls=%async_computation.1 | async-start | bytes 3932160 | tf_op jit(solution)/shard_map/all_gather | solution.py:42
  7.9 425.0 %reduce-scatter.2.cloned.1.call-start = ((), (), s32[]{:S(2)}) async-start(), calls=%async_computation.2 | async-start | bytes 2359296 | tf_op jit(solution)/shard_map/reduce_scatter | solution.py:112
  8.9 44.7 %copy-start.14 = (f32[1,256]{1,0:T(1,128)}, f32[1,256]{1,0:T(1,128)S(1)}, u32[]{:S(2)}) copy-start(f32[1,256]{1,0:T(1,128)S(1)} %get-tuple-element.76) | copy-start | bytes 3076
  8.9 44.7 %copy-start.16 = (f32[1,256]{1,0:T(1,128)}, f32[1,256]{1,0:T(1,128)S(1)}, u32[]{:S(2)}) copy-start(f32[1,256]{1,0:T(1,128)S(1)} %get-tuple-element.77) | copy-start | bytes 3076
  8.9 44.7 %copy-start.18 = (f32[1,256]{1,0:T(1,128)}, f32[1,256]{1,0:T(1,128)S(1)}, u32[]{:S(2)}) copy-start(f32[1,256]{1,0:T(1,128)S(1)} %get-tuple-element.78) | copy-start | bytes 3076
  8.9 44.6 %copy-start.20 = (f32[1,256]{1,0:T(1,128)}, f32[1,256]{1,0:T(1,128)S(1)}, u32[]{:S(2)}) copy-start(f32[1,256]{1,0:T(1,128)S(1)} %get-tuple-element.79) | copy-start | bytes 3076
  44.0 4.7 %collective-permute-start = (bf16[3,256]{1,0:T(4,128)(2,1)S(1)}, bf16[3,256]{1,0:T(4,128)(2,1)S(1)}, u32[]{:S(2)}, u32[]{:S(2)}) collective-permute-start(bf16[3,256]{1,0:T(4,128)(2,1)S(1)} %slice.991), channel_id=1, source_target_pairs={{0,4},{4,8},{8,12},{12,16},{16,20},{20,24},{24,28},{1,5},{5,9},{9,... | collective-permute-start | bytes 4616 | tf_op jit(solution)/shard_map/ppermute | solution.py:14
  48.1 5.4 %copy-start.22 = (f32[256]{0:T(256)}, f32[256]{0:T(256)S(1)}, u32[]{:S(2)}) copy-start(f32[256]{0:T(256)S(1)} %fusion.82) | copy-start | bytes 3076
  49.3 1.4 copy-start.13
  55.6 0.9 copy-start.3
  120.2 27.1 %copy-start.29 = (f32[1,256]{1,0:T(1,128)S(1)}, f32[1,256]{1,0:T(1,128)}, u32[]{:S(2)}) copy-start(f32[1,256]{1,0:T(1,128)} %slice.1054) | copy-start | bytes 3076
  120.2 28.5 %copy-start.28 = (f32[1,256]{1,0:T(1,128)S(1)}, f32[1,256]{1,0:T(1,128)}, u32[]{:S(2)}) copy-start(f32[1,256]{1,0:T(1,128)} %slice.1094) | copy-start | bytes 3076
  134.7 26.4 %copy-start.27 = (f32[1,256]{1,0:T(1,128)S(1)}, f32[1,256]{1,0:T(1,128)}, u32[]{:S(2)}) copy-start(f32[1,256]{1,0:T(1,128)} %slice.1053) | copy-start | bytes 3076
  143.9 20.3 %copy-start.26 = (f32[1,256]{1,0:T(1,128)S(1)}, f32[1,256]{1,0:T(1,128)}, u32[]{:S(2)}) copy-start(f32[1,256]{1,0:T(1,128)} %slice.1093) | copy-start | bytes 3076
  170.8 8.8 %copy-start.25 = (f32[1,256]{1,0:T(1,128)S(1)}, f32[1,256]{1,0:T(1,128)}, u32[]{:S(2)}) copy-start(f32[1,256]{1,0:T(1,128)} %slice.1092) | copy-start | bytes 3076
  177.2 31.2 %copy-start.24 = (f32[1,256]{1,0:T(1,128)S(1)}, f32[1,256]{1,0:T(1,128)}, u32[]{:S(2)}) copy-start(f32[1,256]{1,0:T(1,128)} %slice.1049) | copy-start | bytes 3076
  233.7 5.5 %copy-start.30 = (f32[1,256]{1,0:T(1,128)}, f32[1,256]{1,0:T(1,128)S(1)}, u32[]{:S(2)}) copy-start(f32[1,256]{1,0:T(1,128)S(1)} %broadcast_select_fusion) | copy-start | bytes 3076
  273.3 5.4 %copy-start.8 = (f32[383,256]{1,0:T(8,128)S(1)}, f32[383,256]{1,0:T(8,128)}, u32[]{:S(2)}) copy-start(f32[383,256]{1,0:T(8,128)} %slice.834) | copy-start | bytes 1176580
  285.2 4.5 %copy-start.11 = (f32[191,256]{1,0:T(8,128)S(1)}, f32[191,256]{1,0:T(8,128)}, u32[]{:S(2)}) copy-start(f32[191,256]{1,0:T(8,128)} %slice.773) | copy-start | bytes 586756
  331.3 15.1 %copy-start.2 = (f32[768,256]{1,0:T(8,128)S(1)}, f32[768,256]{1,0:T(8,128)}, u32[]{:S(2)}) copy-start(f32[768,256]{1,0:T(8,128)} %copy.43) | copy-start | bytes 2359300
  331.3 15.1 %copy-start.15 = (f32[1,256]{1,0:T(1,128)S(1)}, f32[1,256]{1,0:T(1,128)}, u32[]{:S(2)}) copy-start(f32[1,256]{1,0:T(1,128)} %copy-done.14) | copy-start | bytes 3076
  331.3 15.1 %copy-start.17 = (f32[1,256]{1,0:T(1,128)S(1)}, f32[1,256]{1,0:T(1,128)}, u32[]{:S(2)}) copy-start(f32[1,256]{1,0:T(1,128)} %copy-done.16) | copy-start | bytes 3076
  331.3 15.1 %copy-start.19 = (f32[1,256]{1,0:T(1,128)S(1)}, f32[1,256]{1,0:T(1,128)}, u32[]{:S(2)}) copy-start(f32[1,256]{1,0:T(1,128)} %copy-done.18) | copy-start | bytes 3076
  331.3 15.1 %copy-start.21 = (f32[1,256]{1,0:T(1,128)S(1)}, f32[1,256]{1,0:T(1,128)}, u32[]{:S(2)}) copy-start(f32[1,256]{1,0:T(1,128)} %copy-done.20) | copy-start | bytes 3076
  331.3 15.1 %copy-start.23 = (f32[256]{0:T(256)S(1)}, f32[256]{0:T(256)}, u32[]{:S(2)}) copy-start(f32[256]{0:T(256)} %copy-done.22) | copy-start | bytes 3076
  331.4 15.1 %copy-start.31 = (f32[1,256]{1,0:T(1,128)S(1)}, f32[1,256]{1,0:T(1,128)}, u32[]{:S(2)}) copy-start(f32[1,256]{1,0:T(1,128)} %copy-done.30) | copy-start | bytes 3076
  351.3 5.8 %copy-start.5 = (f32[768,256]{1,0:T(8,128)S(1)}, f32[768,256]{1,0:T(8,128)}, u32[]{:S(2)}) copy-start(f32[768,256]{1,0:T(8,128)} %get-tuple-element.17) | copy-start | bytes 2359300
  357.1 7.4 %copy-start.4 = (bf16[768,2048]{1,0:T(8,128)(2,1)S(1)}, bf16[768,2048]{1,0:T(8,128)(2,1)}, u32[]{:S(2)}) copy-start(bf16[768,2048]{1,0:T(8,128)(2,1)} %all-gather.5.cloned.1.call-done) | copy-start | bytes 9437188
  358.7 5.5 %collective-permute-start.1 = (f32[3,256]{1,0:T(4,128)S(1)}, f32[3,256]{1,0:T(4,128)S(1)}, u32[]{:S(2)}, u32[]{:S(2)}) collective-permute-start(f32[3,256]{1,0:T(4,128)S(1)} %slice.1134), channel_id=1, source_target_pairs={{4,0},{8,4},{12,8},{16,12},{20,16},{24,20},{28,24},{5,1},{9,5},{13... | collective-permute-start | bytes 9224 | tf_op jit(solution)/shard_map/ppermute | solution.py:14
  364.2 70.5 %copy-start.1 = (bf16[2048,256]{1,0:T(8,128)(2,1)S(1)}, bf16[2048,256]{1,0:T(8,128)(2,1)}, u32[]{:S(2)}) copy-start(bf16[2048,256]{1,0:T(8,128)(2,1)} %param.10) | copy-start | bytes 3145732
  364.6 2.3 copy-start.9
  (4 other events, 3.0 us)
Sparse Core Ops, SparseCore 0:
  9.6 31.2 all-gather.4
  367.0 65.8 reduce-scatter.1
where the time goes:
time: 447 us; the launch traced here: 442 us
  local copies, waits for them, and re-layouts  172 us (38%)
  waiting for transfers between devices  103 us (23%)
  other arithmetic  73.5 us (16%)
  blocking collectives  56.1 us (13%)
  matrix products  16.1 us (4%)
  between operations  15.5 us (3%)
  starting transfers between devices  4.75 us (1%)
    reduce_scatter x1, waiting for transfers between devices, per_device(): lax.psum_scatter(lax.dot_general(gathered, d_proj, (((0,), (0,)), ((), ()...  66 us
    slice x63, local copies, waits for them, and re-layouts, per_device(): lax.associative_scan(combine, (decay_rate, drive), axis=0)  51 us
    slice x69, local copies, waits for them, and re-layouts, per_device(): lax.associative_scan(combine, (shifted, drive_grad), reverse=True, axis=0)  41.5 us
    pad x34, local copies, waits for them, and re-layouts, per_device(): lax.associative_scan(combine, (decay_rate, drive), axis=0)  40.1 us
    all_gather x1, waiting for transfers between devices, per_device(): gathered = lax.all_gather(tokens, 'tp', axis=1, tiled=True)  31.9 us
    all_gather x1, blocking collectives, per_device(): lax.all_gather(span_state[None], 'sp', axis=0, tiled=True)  21.3 us
    all_gather x1, blocking collectives, per_device(): lax.all_gather(span_grad[None], 'sp', axis=0, tiled=True)  18.3 us
    add x22, other arithmetic, combine(): return (earlier[0] * later[0], later[0] * earlier[1] + later[1])  17.5 us
  transfers between devices with their start and end apart: 4, of which 4 were waited for; matrix products, arithmetic and copies ran while one was open for 0% of the time, Pallas kernels for 0%

commit v1 on v0

--- a/solution.py
+++ b/solution.py
@@ -39,7 +39,12 @@
     row_count = tokens.shape[0]
     chan_width = proj_weight.shape[1]
     block_count = chan_width // BLOCK
-    gathered = lax.all_gather(tokens, "tp", axis=1, tiled=True)
+    ring = [tokens]
+    for hop in range(3):
+        ring.append(lax.ppermute(ring[-1], "tp", [(dev, (dev + 1) % 4) for dev in range(4)]))
+    gathered = jnp.roll(
+        jnp.concatenate(ring[::-1], axis=1), (lax.axis_index("tp") + 1) * ring[0].shape[1], axis=1
+    )
     projected = jnp.dot(gathered, proj_weight, preferred_element_type=jnp.float32).astype(
         jnp.bfloat16
     )

time: 447 us -> 460 us (1.029)
  local copies, waits for them, and re-layouts: 172 us -> 182 us
    ppermute x0 -> x3, waiting for transfers between devices: none -> 33.7 us  [per_device(): lax.ppermute(ring[-1], 'tp', [(dev, (dev + 1) % 4) for dev in range(4)])]
    all_gather x1 -> x0, waiting for transfers between devices: 31.9 us -> none  [per_device(): gathered = lax.all_gather(tokens, 'tp', axis=1, tiled=True)]
    unnamed x68 -> x66, local copies, waits for them, and re-layouts: 5.82 us -> 10.7 us
    rev x2, local copies, waits for them, and re-layouts: 7.14 us -> 12 us  [per_device(): lax.associative_scan(combine, (shifted, drive_grad), reverse=True, axis=0)]
  transfers between devices with their start and end apart: 4 -> 6, of which waited for: 4 -> 6; matrix products, arithmetic and copies ran while one was open for 0% -> 0% of each run, Pallas kernels for 0% -> 0%
where the time goes in v1:
time: 460 us; the launch traced here: 454 us
  local copies, waits for them, and re-layouts  182 us (40%)
  waiting for transfers between devices  105 us (23%)
  other arithmetic  73.4 us (16%)
  blocking collectives  56.3 us (12%)
  matrix products  15.9 us (3%)
  between operations  15.5 us (3%)
  starting transfers between devices  6.15 us (1%)
    reduce_scatter x1, waiting for transfers between devices, per_device(): lax.psum_scatter(lax.dot_general(gathered, d_proj, (((0,), (0,)), ((), ()...  66 us
    slice x63, local copies, waits for them, and re-layouts, per_device(): lax.associative_scan(combine, (decay_rate, drive), axis=0)  50.5 us
    slice x69, local copies, waits for them, and re-layouts, per_device(): lax.associative_scan(combine, (shifted, drive_grad), reverse=True, axis=0)  40.9 us
    pad x34, local copies, waits for them, and re-layouts, per_device(): lax.associative_scan(combine, (decay_rate, drive), axis=0)  40.2 us
    ppermute x3, waiting for transfers between devices, per_device(): lax.ppermute(ring[-1], 'tp', [(dev, (dev + 1) % 4) for dev in range(4)])  33.7 us
    all_gather x1, blocking collectives, per_device(): lax.all_gather(span_state[None], 'sp', axis=0, tiled=True)  21.6 us
    all_gather x1, blocking collectives, per_device(): lax.all_gather(span_grad[None], 'sp', axis=0, tiled=True)  18.3 us
    add x22, other arithmetic, combine(): return (earlier[0] * later[0], later[0] * earlier[1] + later[1])  17.5 us
  transfers between devices with their start and end apart: 6, of which 6 were waited for; matrix products, arithmetic and copies ran while one was open for 0% of the time, Pallas kernels for 0%

profile of v1, /device:TPU:0, one launch (start us, length us, event | category | flops | bytes accessed | tf_op | source)
XLA Modules:
  0.0 454.0 jit_solution(11432817123174443376)
XLA Ops:
  7.8 11.8 %collective-permute-done = bf16[768,512]{1,0:T(8,128)(2,1)S(1)} collective-permute-done((bf16[768,512]{1,0:T(8,128)(2,1)}, bf16[768,512]{1,0:T(8,128)(2,1)S(1)}, u32[]{:S(2)}, u32[]{:S(2)}) %collective-permute-start) | collective-permute-done | bytes 786464 | tf_op jit(solution)/shard_map/ppermute | solution.py:44
  19.6 11.4 %collective-permute-done.1 = bf16[768,512]{1,0:T(8,128)(2,1)S(1)} collective-permute-done((bf16[768,512]{1,0:T(8,128)(2,1)S(1)}, bf16[768,512]{1,0:T(8,128)(2,1)S(1)}, u32[]{:S(2)}, u32[]{:S(2)}) %collective-permute-start.1) | collective-permute-done | bytes 786464 | tf_op jit(solution)/shard_map/ppermute | solution.py:44
  32.0 10.6 %collective-permute-done.2 = bf16[768,512]{1,0:T(8,128)(2,1)} collective-permute-done((bf16[768,512]{1,0:T(8,128)(2,1)S(1)}, bf16[768,512]{1,0:T(8,128)(2,1)}, u32[]{:S(2)}, u32[]{:S(2)}) %collective-permute-start.2) | collective-permute-done | bytes 786464 | tf_op jit(solution)/shard_map/ppermute | solution.py:44
  50.4 4.2 collective-permute-start.3
  64.4 3.2 slice.964
  67.5 3.2 slice.924
  70.7 3.2 slice.923
  190.7 3.0 pad.337
  194.4 21.6 %all-gather.2 = f32[8,1,256]{2,1,0:T(1,128)S(1)} all-gather(f32[1,1,256]{2,1,0:T(1,128)S(1)} %add_bitcast_fusion), channel_id=1, replica_groups=mesh['sp'=8,'tp'=4] {'sp'}, dimensions={0}, use_global_device_ids=true | all-gather | bytes 9216 | tf_op jit(solution)/shard_map/all_gather | solution.py:86
  217.8 2.9 pad.312
  220.7 2.9 pad.313
  224.3 16.5 %all-gather.1 = f32[8,1,256]{2,1,0:T(1,128)S(1)} all-gather(f32[1,1,256]{2,1,0:T(1,128)S(1)} %add_bitcast_fusion.1), channel_id=1, replica_groups=mesh['sp'=8,'tp'=4] {'sp'}, dimensions={0}, use_global_device_ids=true | all-gather | bytes 9216 | tf_op jit(solution)/shard_map/all_gather | solution.py:85
  241.3 5.5 %fusion.24 = (bf16[768,256]{1,0:T(8,128)(2,1)}, f32[768,256]{1,0:T(8,128)}, f32[768,256]{1,0:T(8,128)S(1)}) fusion(bf16[768,256]{1,0:T(8,128)(2,1)} %param.15, f32[256]{0:T(256)S(1)} %bitcast.84, f32[768,256]{1,0:T(8,128)} %pad.312, f32[768,256]{1,0:T(8,128)} %pad.313, f32[768,256]{1,0:T(8,128)} %pad.336, f32[768,256]{1,0:T(8,128)} %pad.337, ...), kind=kOutput, calls=%fused_computation.34 | convolution fusion | flops 811204608 | bytes 9700356 | tf_op jit(solution)/shard_map/dot_general | solution.py:51
  247.7 3.2 slice.834
  250.9 3.1 slice.768
  254.0 3.1 slice.766
  261.7 3.9 slice.767
  265.5 3.9 slice.769
  269.4 3.9 slice.772
  273.3 3.8 slice.765
  283.7 4.0 slice.835
  287.7 3.9 slice.763
  311.2 3.0 pad.277
  317.3 18.3 %all-gather = f32[8,1,256]{2,1,0:T(1,128)S(1)} all-gather(f32[1,1,256]{2,1,0:T(1,128)S(1)} %fusion.100), channel_id=1, replica_groups=mesh['sp'=8,'tp'=4] {'sp'}, dimensions={0}, use_global_device_ids=true | all-gather | bytes 9216 | tf_op jit(solution)/shard_map/all_gather | solution.py:87
  337.8 5.1 %rev.6 = f32[768,256]{1,0:T(8,128)S(1)} reverse(f32[768,256]{1,0:T(8,128)} %add.563), dimensions={0} | reverse | bytes 1572864 | tf_op jit(solution)/shard_map/rev | solution.py:78
  343.3 2.9 pad.294
  346.1 3.0 pad.295
  351.5 6.8 %rev.14 = f32[768,256]{1,0:T(8,128)} reverse(f32[768,256]{1,0:T(8,128)} %add.572), dimensions={0} | reverse | bytes 1572864 | tf_op jit(solution)/shard_map/rev | solution.py:78
  358.4 3.7 fusion.21
  372.0 4.2 collective-permute-done.4
  376.6 4.5 fusion
  381.1 66.0 %reduce-scatter.2.cloned.1.call-done = f32[256,256]{1,0:T(8,128)} async-done(((f32[2048,256]{1,0:T(8,128)}), f32[256,256]{1,0:T(8,128)}) %reduce-scatter.2.cloned.1.call-update) | async-done | bytes 262160 | tf_op jit(solution)/shard_map/reduce_scatter | solution.py:117
  (441 shorter events, 188.5 us)
Async XLA Ops:
  7.2 234.1 %copy-start = (bf16[2048,256]{1,0:T(8,128)(2,1)S(1)}, bf16[2048,256]{1,0:T(8,128)(2,1)}, u32[]{:S(2)}) copy-start(bf16[2048,256]{1,0:T(8,128)(2,1)} %param.10) | copy-start | bytes 3145732
  7.2 39.4 %copy-start.4 = (bf16[768,512]{1,0:T(8,128)(2,1)S(1)}, bf16[768,512]{1,0:T(8,128)(2,1)}, u32[]{:S(2)}) copy-start(bf16[768,512]{1,0:T(8,128)(2,1)} %param.8) | copy-start | bytes 2359300
  7.2 439.9 %reduce-scatter.2.cloned.1.call-start = ((), (), s32[]{:S(2)}) async-start(), calls=%async_computation.1 | async-start | bytes 2359296 | tf_op jit(solution)/shard_map/reduce_scatter | solution.py:117
  7.2 12.3 %collective-permute-start = (bf16[768,512]{1,0:T(8,128)(2,1)}, bf16[768,512]{1,0:T(8,128)(2,1)S(1)}, u32[]{:S(2)}, u32[]{:S(2)}) collective-permute-start(bf16[768,512]{1,0:T(8,128)(2,1)} %param.8), channel_id=1, source_target_pairs={{0,1},{1,2},{2,3},{3,0},{4,5},{5,6},{6,7},{7,4},{8,9},{9,10},{10,1... | collective-permute-start | bytes 2359304 | tf_op jit(solution)/shard_map/ppermute | solution.py:44
  19.6 11.4 %collective-permute-start.1 = (bf16[768,512]{1,0:T(8,128)(2,1)S(1)}, bf16[768,512]{1,0:T(8,128)(2,1)S(1)}, u32[]{:S(2)}, u32[]{:S(2)}) collective-permute-start(bf16[768,512]{1,0:T(8,128)(2,1)S(1)} %collective-permute-done), channel_id=1, source_target_pairs={{0,1},{1,2},{2,3},{3,0},{4,5},{5,6},{6,7},{7,4},{8,9},{9,10},{10,1... | collective-permute-start | bytes 2359304 | tf_op jit(solution)/shard_map/ppermute | solution.py:44
  31.0 11.5 %collective-permute-start.2 = (bf16[768,512]{1,0:T(8,128)(2,1)S(1)}, bf16[768,512]{1,0:T(8,128)(2,1)}, u32[]{:S(2)}, u32[]{:S(2)}) collective-permute-start(bf16[768,512]{1,0:T(8,128)(2,1)S(1)} %collective-permute-done.1), channel_id=1, source_target_pairs={{0,1},{1,2},{2,3},{3,0},{4,5},{5,6},{6,7},{7,4},{8,9},{9,10},{10,1... | collective-permute-start | bytes 2359304 | tf_op jit(solution)/shard_map/ppermute | solution.py:44
  31.9 28.9 %copy-start.13 = (f32[1,256]{1,0:T(1,128)}, f32[1,256]{1,0:T(1,128)S(1)}, u32[]{:S(2)}) copy-start(f32[1,256]{1,0:T(1,128)S(1)} %get-tuple-element.67) | copy-start | bytes 3076
  31.9 28.9 %copy-start.15 = (f32[1,256]{1,0:T(1,128)}, f32[1,256]{1,0:T(1,128)S(1)}, u32[]{:S(2)}) copy-start(f32[1,256]{1,0:T(1,128)S(1)} %get-tuple-element.68) | copy-start | bytes 3076
  31.9 28.9 %copy-start.17 = (f32[1,256]{1,0:T(1,128)}, f32[1,256]{1,0:T(1,128)S(1)}, u32[]{:S(2)}) copy-start(f32[1,256]{1,0:T(1,128)S(1)} %get-tuple-element.69) | copy-start | bytes 3076
  31.9 28.9 %copy-start.19 = (f32[1,256]{1,0:T(1,128)}, f32[1,256]{1,0:T(1,128)S(1)}, u32[]{:S(2)}) copy-start(f32[1,256]{1,0:T(1,128)S(1)} %get-tuple-element.70) | copy-start | bytes 3076
  31.9 17.4 %copy-start.27 = (bf16[2048,256]{1,0:T(8,128)(2,1)S(1)}, bf16[2048,256]{1,0:T(8,128)(2,1)}, u32[]{:S(2)}) copy-start(bf16[2048,256]{1,0:T(8,128)(2,1)} %param.9) | copy-start | bytes 3145732
  46.7 2.6 copy-start.12
  50.4 5.5 %collective-permute-start.3 = (bf16[3,256]{1,0:T(4,128)(2,1)S(1)}, bf16[3,256]{1,0:T(4,128)(2,1)S(1)}, u32[]{:S(2)}, u32[]{:S(2)}) collective-permute-start(bf16[3,256]{1,0:T(4,128)(2,1)S(1)} %slice.991), channel_id=1, source_target_pairs={{0,4},{4,8},{8,12},{12,16},{16,20},{20,24},{24,28},{1,5},{5,9},{9,... | collective-permute-start | bytes 4616 | tf_op jit(solution)/shard_map/ppermute | solution.py:14
  55.4 5.4 %copy-start.21 = (f32[256]{0:T(256)}, f32[256]{0:T(256)S(1)}, u32[]{:S(2)}) copy-start(f32[256]{0:T(256)S(1)} %fusion.97) | copy-start | bytes 3076
  56.5 1.4 copy-start.10
  62.9 0.9 copy-start.3
  81.0 0.7 copy-start.6
  127.0 41.3 %copy-start.26 = (f32[1,256]{1,0:T(1,128)S(1)}, f32[1,256]{1,0:T(1,128)}, u32[]{:S(2)}) copy-start(f32[1,256]{1,0:T(1,128)} %slice.1053) | copy-start | bytes 3076
  127.0 44.5 %copy-start.25 = (f32[1,256]{1,0:T(1,128)S(1)}, f32[1,256]{1,0:T(1,128)}, u32[]{:S(2)}) copy-start(f32[1,256]{1,0:T(1,128)} %slice.1093) | copy-start | bytes 3076
  156.0 31.1 %copy-start.24 = (f32[1,256]{1,0:T(1,128)S(1)}, f32[1,256]{1,0:T(1,128)}, u32[]{:S(2)}) copy-start(f32[1,256]{1,0:T(1,128)} %slice.1092) | copy-start | bytes 3076
  168.3 47.7 %copy-start.23 = (f32[1,256]{1,0:T(1,128)S(1)}, f32[1,256]{1,0:T(1,128)}, u32[]{:S(2)}) copy-start(f32[1,256]{1,0:T(1,128)} %slice.1049) | copy-start | bytes 3076
  246.8 0.9 copy-start.7
  311.2 47.1 %copy-start.2 = (f32[768,256]{1,0:T(8,128)S(1)}, f32[768,256]{1,0:T(8,128)}, u32[]{:S(2)}) copy-start(f32[768,256]{1,0:T(8,128)} %copy.41) | copy-start | bytes 2359300
  311.2 47.1 %copy-start.14 = (f32[1,256]{1,0:T(1,128)S(1)}, f32[1,256]{1,0:T(1,128)}, u32[]{:S(2)}) copy-start(f32[1,256]{1,0:T(1,128)} %copy-done.13) | copy-start | bytes 3076
  311.2 47.1 %copy-start.16 = (f32[1,256]{1,0:T(1,128)S(1)}, f32[1,256]{1,0:T(1,128)}, u32[]{:S(2)}) copy-start(f32[1,256]{1,0:T(1,128)} %copy-done.15) | copy-start | bytes 3076
  311.2 47.1 %copy-start.18 = (f32[1,256]{1,0:T(1,128)S(1)}, f32[1,256]{1,0:T(1,128)}, u32[]{:S(2)}) copy-start(f32[1,256]{1,0:T(1,128)} %copy-done.17) | copy-start | bytes 3076
  311.2 47.1 %copy-start.20 = (f32[1,256]{1,0:T(1,128)S(1)}, f32[1,256]{1,0:T(1,128)}, u32[]{:S(2)}) copy-start(f32[1,256]{1,0:T(1,128)} %copy-done.19) | copy-start | bytes 3076
  311.2 47.1 %copy-start.22 = (f32[256]{0:T(256)S(1)}, f32[256]{0:T(256)}, u32[]{:S(2)}) copy-start(f32[256]{0:T(256)} %copy-done.21) | copy-start | bytes 3076
  362.1 6.9 %copy-start.5 = (f32[768,256]{1,0:T(8,128)S(1)}, f32[768,256]{1,0:T(8,128)}, u32[]{:S(2)}) copy-start(f32[768,256]{1,0:T(8,128)} %get-tuple-element.8) | copy-start | bytes 2359300
  369.0 78.2 %copy-start.1 = (bf16[2048,256]{1,0:T(8,128)(2,1)S(1)}, bf16[2048,256]{1,0:T(8,128)(2,1)}, u32[]{:S(2)}) copy-start(bf16[2048,256]{1,0:T(8,128)(2,1)} %param.10) | copy-start | bytes 3145732
  370.7 5.5 %collective-permute-start.4 = (f32[3,256]{1,0:T(4,128)S(1)}, f32[3,256]{1,0:T(4,128)S(1)}, u32[]{:S(2)}, u32[]{:S(2)}) collective-permute-start(f32[3,256]{1,0:T(4,128)S(1)} %slice.1134), channel_id=1, source_target_pairs={{4,0},{8,4},{12,8},{16,12},{20,16},{24,20},{28,24},{5,1},{9,5},{13... | collective-permute-start | bytes 9224 | tf_op jit(solution)/shard_map/ppermute | solution.py:14
  376.6 70.5 %copy-start.11 = (bf16[768,256]{1,0:T(8,128)(2,1)}, bf16[768,256]{1,0:T(8,128)(2,1)S(1)}, u32[]{:S(2)}) copy-start(bf16[768,256]{1,0:T(8,128)(2,1)S(1)} %fusion.29) | copy-start | bytes 1179652
  (2 other events, 1.3 us)
Sparse Core Ops, SparseCore 0:
  381.2 65.8 reduce-scatter.1
